TPU v7x, 32 devices: a whole 2x2x4 slice. The times are simulated.
32 devices in a mesh: kv: 8 (over z, x), tp: 4 (over y, core).
Axes of the slice: x: 2, y: 2, z: 4, core: 2. Of those that a mesh axis runs over, the one named last changes fastest.
Arguments:
- tokens: bfloat16 [8192, 2048], P('kv'), may hold values from -72 to 72
- query_weight: bfloat16 [2048, 2048], P(None, 'tp'), may hold values from -0.125 to 0.125
- key_projection_matrix: bfloat16 [2048, 1024], P(None, 'tp'), may hold values from -0.125 to 0.125
- value_projection_matrix: bfloat16 [2048, 1024], P(None, 'tp'), may hold values from -0.125 to 0.125
- out_weight: bfloat16 [2048, 2048], P('tp'), may hold values from -1.5 to 1.5
- chosen: int32 [64, 12], P('kv'), may hold values from -1 to 255, as said below
Outputs:
- layer_out: bfloat16 [8192, 2048], P(('kv', 'tp'))
Inputs may be any that keep to these rules, and one draw needn't show every extreme that they name: `chosen`: positions are grouped in consecutive groups of 1024. The blocks named in one row lie in distinct groups, all earlier than the group of the row's query block; a query block in group g has exactly min(12, g) entries that are not -1, first in its row, and the rest are -1. So the query blocks of one group name at most 8 blocks of any one other group, and in every draw some group's query blocks all name blocks of one same earlier group.
All inputs are finite; a program needn't handle non-finite values.
Results may differ from a plain program's by a relative error of at most 0.014.
The roundings to bfloat16 on the way count: a program that leaves them out, or rounds other values in their place, can miss the bound.
Values may be sent and summed in bfloat16 or wider, within the bound.
A program may use at most 64 MiB of HBM per device.

v0:
```python
import jax
import jax.numpy as jnp
from jax import lax
from jax.sharding import PartitionSpec as P

HEAD_SIZE = 128
QUERY_BLOCK_SPAN = 128
KEY_BLOCK_SPAN = 32
NFAR = 12


def shards(
    tokens, query_weight, key_projection_matrix, value_projection_matrix, out_weight, chosen
):
    tok_rows = tokens.shape[0]
    kv_width = key_projection_matrix.shape[1]
    kv_heads = kv_width // HEAD_SIZE
    q_heads = query_weight.shape[1] // HEAD_SIZE
    grouped_head_index = q_heads // kv_heads
    query_blocks = tok_rows // QUERY_BLOCK_SPAN
    blocked_keys = tok_rows // KEY_BLOCK_SPAN
    queries = jnp.dot(tokens, query_weight, preferred_element_type=jnp.float32).astype(jnp.bfloat16)
    key_vectors = jnp.dot(tokens, key_projection_matrix, preferred_element_type=jnp.float32).astype(
        jnp.bfloat16
    )
    value_vectors = jnp.dot(
        tokens, value_projection_matrix, preferred_element_type=jnp.float32
    ).astype(jnp.bfloat16)
    my_index = lax.axis_index("kv")
    key_rows = key_vectors.reshape(blocked_keys, KEY_BLOCK_SPAN, kv_width)
    value_rows = value_vectors.reshape(blocked_keys, KEY_BLOCK_SPAN, kv_width)
    all_lists = lax.all_gather(chosen, "kv", axis=0, tiled=True)
    peer_count = all_lists.shape[0] // query_blocks
    asked_ids = all_lists.reshape(peer_count, query_blocks, NFAR)
    is_mine = (asked_ids >= 0) & (asked_ids // blocked_keys == my_index)
    wanted = jnp.sum(jnp.where(is_mine, asked_ids - my_index * blocked_keys, 0), axis=2)
    received = (
        lax.all_to_all(key_rows[wanted], "kv", split_axis=0, concat_axis=0, tiled=True),
        lax.all_to_all(value_rows[wanted], "kv", split_axis=0, concat_axis=0, tiled=True),
    )
    owners = jnp.where(chosen >= 0, chosen // blocked_keys, 0)
    block_slot = jnp.arange(query_blocks, dtype=jnp.int32)[:, None]
    far_keys = received[0][owners, block_slot]
    far_values = received[1][owners, block_slot]
    listed_keys = QUERY_BLOCK_SPAN + NFAR * KEY_BLOCK_SPAN
    row_offset = my_index * tok_rows
    query_pos = row_offset + jnp.arange(tok_rows, dtype=jnp.int32).reshape(
        query_blocks, QUERY_BLOCK_SPAN
    )
    far_pos = (
        jnp.maximum(chosen, 0)[:, :, None] * KEY_BLOCK_SPAN
        + jnp.arange(KEY_BLOCK_SPAN, dtype=jnp.int32)
    ).reshape(query_blocks, NFAR * KEY_BLOCK_SPAN)
    far_ok = jnp.broadcast_to(
        (chosen >= 0)[:, :, None], (query_blocks, NFAR, KEY_BLOCK_SPAN)
    ).reshape(query_blocks, NFAR * KEY_BLOCK_SPAN)
    key_pos = jnp.concatenate([query_pos, far_pos], axis=1)
    key_ok = jnp.concatenate(
        [jnp.ones((query_blocks, QUERY_BLOCK_SPAN), dtype=bool), far_ok], axis=1
    )
    allowed = key_ok[:, None, :] & (key_pos[:, None, :] <= query_pos[:, :, None])
    all_keys = jnp.concatenate(
        [
            key_vectors.reshape(query_blocks, QUERY_BLOCK_SPAN, kv_width),
            far_keys.reshape(query_blocks, NFAR * KEY_BLOCK_SPAN, kv_width),
        ],
        axis=1,
    )
    all_values = jnp.concatenate(
        [
            value_vectors.reshape(query_blocks, QUERY_BLOCK_SPAN, kv_width),
            far_values.reshape(query_blocks, NFAR * KEY_BLOCK_SPAN, kv_width),
        ],
        axis=1,
    )
    grouped = queries.reshape(
        query_blocks, QUERY_BLOCK_SPAN, kv_heads, grouped_head_index, HEAD_SIZE
    )
    scores = jnp.einsum(
        "bqgrd,bkgd->bgrqk",
        grouped,
        all_keys.reshape(query_blocks, listed_keys, kv_heads, HEAD_SIZE),
        preferred_element_type=jnp.float32,
    ) * HEAD_SIZE ** (-0.5)
    scores = jnp.where(allowed[:, None, None], scores, -jnp.inf)
    row_max = jnp.max(scores, axis=-1, keepdims=True)
    exp_scores = jnp.exp(scores - row_max)
    row_sum = jnp.sum(exp_scores, axis=-1, keepdims=True)
    weights = (exp_scores / row_sum).astype(jnp.bfloat16)
    mixed = jnp.einsum(
        "bgrqk,bkgd->bqgrd",
        weights,
        all_values.reshape(query_blocks, listed_keys, kv_heads, HEAD_SIZE),
        preferred_element_type=jnp.float32,
    )
    mixed = mixed.astype(jnp.bfloat16).reshape(tok_rows, q_heads * HEAD_SIZE)
    return lax.psum_scatter(
        jnp.dot(mixed, out_weight, preferred_element_type=jnp.float32).astype(jnp.bfloat16),
        "tp",
        scatter_dimension=0,
        tiled=True,
    )


def solution(mesh):
    return jax.shard_map(
        shards,
        mesh=mesh,
        in_specs=(
            P("kv", None),
            P(None, "tp"),
            P(None, "tp"),
            P(None, "tp"),
            P("tp", None),
            P("kv", None),
        ),
        out_specs=P(("kv", "tp"), None),
        check_vma=False,
    )
```

profile of v0, /device:TPU:0, one launch (start us, length us, event | category | flops | bytes accessed | tf_op | source)
XLA Modules:
  0.0 185.1 jit_solution(7131754344731125927)
XLA Ops:
  6.5 0.0 copy-start
  6.5 32.7 %all_gather.3 = s32[64,12]{1,0:T(8,128)S(1)} all-gather(s32[8,12]{1,0:T(8,128)} %param.11), channel_id=1, replica_groups=mesh['kv'=8,'tp'=4] {'kv'}, dimensions={0}, use_global_device_ids=true | all-gather | bytes 3456 | tf_op jit(solution)/shard_map/all_gather | solution.py:32
  39.2 0.1 select_reduce_fusion
  39.3 0.1 reduce_sum.21
  39.4 0.1 reshape.100
  39.5 3.7 %convolution_convert_fusion.2 = bf16[1024,256]{1,0:T(8,128)(2,1)S(1)} fusion(bf16[1024,2048]{1,0:T(8,128)(2,1)} %param.6, bf16[2048,256]{1,0:T(8,128)(2,1)} %param.8), kind=kOutput, calls=%fused_computation.25 | convolution fusion | flops 1074003968 | bytes 5767168 | tf_op jit(solution)/shard_map/dot_general | solution.py:23
  43.3 0.0 copy-start.1
  43.3 1.6 gather_fusion.2
  44.9 0.0 copy-done.1
  44.9 5.5 %all-to-all-start.1 = ((bf16[8,8,32,256]{3,2,1,0:T(8,128)(2,1)}), bf16[8,8,32,256]{3,2,1,0:T(8,128)(2,1)S(1)}, u32[]{:S(2)}, u32[]{:S(2)}) async-start(bf16[8,8,32,256]{3,2,1,0:T(8,128)(2,1)} %bitcast.56), calls=%async_computation.1 | async-start | bytes 2097152 | tf_op jit(solution)/shard_map/all_to_all | solution.py:38
  50.3 0.0 copy-start.6
  50.3 4.5 %convolution_convert_fusion.3 = bf16[1024,256]{1,0:T(8,128)(2,1)} fusion(bf16[1024,2048]{1,0:T(8,128)(2,1)} %param.6, bf16[2048,256]{1,0:T(8,128)(2,1)} %param.9), kind=kOutput, calls=%fused_computation.26 | convolution fusion | flops 1074003968 | bytes 5767168 | tf_op jit(solution)/shard_map/dot_general | solution.py:26
  54.9 2.6 %gather_fusion = bf16[64,32,256]{2,1,0:T(8,128)(2,1)} fusion(bf16[32,32,256]{2,1,0:T(8,128)(2,1)} %bitcast.54, s32[1024]{0:T(1024)S(1)} %pad_clamp_fusion), kind=kCustom, calls=%fused_computation | custom fusion | bytes 2097408 | tf_op jit(solution)/shard_map/gather | solution.py:39
  57.5 12.4 %all-to-all-done.1 = bf16[8,8,32,256]{3,2,1,0:T(8,128)(2,1)S(1)} async-done(((bf16[8,8,32,256]{3,2,1,0:T(8,128)(2,1)}), bf16[8,8,32,256]{3,2,1,0:T(8,128)(2,1)S(1)}, u32[]{:S(2)}, u32[]{:S(2)}) %all-to-all-start.1) | async-done | bytes 1048608 | tf_op jit(solution)/shard_map/all_to_all | solution.py:38
  70.0 4.2 %all-to-all-start = ((bf16[8,8,32,256]{3,2,1,0:T(8,128)(2,1)}), bf16[8,8,32,256]{3,2,1,0:T(8,128)(2,1)}, u32[]{:S(2)}, u32[]{:S(2)}) async-start(bf16[8,8,32,256]{3,2,1,0:T(8,128)(2,1)} %bitcast.55), calls=%async_computation | async-start | bytes 2097152 | tf_op jit(solution)/shard_map/all_to_all | solution.py:39
  74.2 0.2 reduce-scatter.2.cloned.1.call-start
  74.4 0.0 copy-done.6
  74.5 2.0 %concatenate.32 = bf16[8,128,2,128]{3,2,1,0:T(2,128)(2,1)} reshape(bf16[1024,256]{1,0:T(8,128)(2,1)} %copy-done.1) | data formatting | bytes 1048576 | tf_op jit(solution)/shard_map/concatenate | solution.py:62
  76.4 1.9 %concatenate.26 = bf16[8,128,2,128]{3,2,1,0:T(2,128)(2,1)} reshape(bf16[1024,256]{1,0:T(8,128)(2,1)} %convolution_convert_fusion.3) | data formatting | bytes 1048576 | tf_op jit(solution)/shard_map/concatenate | solution.py:69
  78.4 0.1 reshape.106
  78.4 2.0 %copy.13 = bf16[8,128,2,128]{3,1,2,0:T(8,128)(2,1)} copy(bf16[8,128,2,128]{3,2,1,0:T(2,128)(2,1)} %concatenate.32) | data formatting | bytes 1048576 | tf_op jit(solution)/shard_map/concatenate | solution.py:62
  80.4 6.2 %convolution_convert_fusion.1 = bf16[1024,512]{1,0:T(8,128)(2,1)} fusion(bf16[1024,2048]{1,0:T(8,128)(2,1)} %param.6, bf16[2048,512]{1,0:T(8,128)(2,1)} %param.7), kind=kOutput, calls=%fused_computation.23 | convolution fusion | flops 2148007936 | bytes 7340032 | tf_op jit(solution)/shard_map/dot_general | solution.py:22
  86.6 2.2 %reshape.96 = bf16[8,128,2,2,128]{4,3,2,1,0:T(2,128)(2,1)} reshape(bf16[1024,512]{1,0:T(8,128)(2,1)} %convolution_convert_fusion.1) | data formatting | bytes 2097152 | tf_op jit(solution)/shard_map/reshape | solution.py:76
  88.8 0.1 add.61
  88.8 0.1 add.62
  88.9 0.1 add.64
  89.0 0.1 broadcast_in_dim.20
  89.1 0.1 reshape.91
  89.2 2.0 %copy.11 = bf16[8,128,2,128]{1,3,2,0:T(8,128)(2,1)} copy(bf16[8,128,2,128]{3,2,1,0:T(2,128)(2,1)} %concatenate.26) | data formatting | bytes 1048576 | tf_op jit(solution)/shard_map/concatenate | solution.py:69
  91.2 2.4 %compare_and_fusion = pred[8,128,512]{1,2,0:T(8,128)(4,1)} fusion(s32[8,128]{1,0:T(8,128)S(1)} %add_add_fusion, s32[8,512]{1,0:T(8,128)S(1)} %pad_add_fusion, pred[8,512]{1,0:T(8,128)(4,1)S(1)} %concatenate.30), kind=kLoop, calls=%fused_computation.21 | loop fusion | flops 1048576 | bytes 548864 | tf_op jit(solution)/shard_map/and | solution.py:61
  93.6 2.3 %gather_fusion.3 = bf16[96,32,256]{2,1,0:T(8,128)(2,1)} fusion(bf16[8,8,32,256]{3,2,1,0:T(8,128)(2,1)S(1)} %all-to-all-done.1, s32[96]{0:T(128)S(1)} %reshape.106), kind=kCustom, calls=%fused_computation.3 | custom fusion | bytes 3146496 | tf_op jit(solution)/shard_map/gather | solution.py:43
  95.9 3.5 %concatenate.33 = bf16[8,384,2,128]{3,2,1,0:T(2,128)(2,1)} reshape(bf16[96,32,256]{2,1,0:T(8,128)(2,1)} %gather_fusion.3) | data formatting | bytes 3145728 | tf_op jit(solution)/shard_map/concatenate | solution.py:62
  99.4 2.9 %copy.14 = bf16[8,384,2,128]{3,1,2,0:T(8,128)(2,1)} copy(bf16[8,384,2,128]{3,2,1,0:T(2,128)(2,1)} %concatenate.33) | data formatting | bytes 3145728 | tf_op jit(solution)/shard_map/concatenate | solution.py:62
  102.3 0.0 copy-start.2
  102.3 0.0 all-to-all-done
  102.3 3.6 %gather_fusion.1 = bf16[96,32,256]{2,1,0:T(8,128)(2,1)} fusion(bf16[8,8,32,256]{3,2,1,0:T(8,128)(2,1)} %all-to-all-done, s32[96]{0:T(128)S(1)} %reshape.106), kind=kCustom, calls=%fused_computation.1 | custom fusion | bytes 3146496 | tf_op jit(solution)/shard_map/gather | solution.py:44
  106.0 3.5 %concatenate.28 = bf16[8,384,2,128]{3,2,1,0:T(2,128)(2,1)} reshape(bf16[96,32,256]{2,1,0:T(8,128)(2,1)} %gather_fusion.1) | data formatting | bytes 3145728 | tf_op jit(solution)/shard_map/concatenate | solution.py:69
  109.5 4.9 %copy.12 = bf16[8,384,2,128]{1,3,2,0:T(8,128)(2,1)} copy(bf16[8,384,2,128]{3,2,1,0:T(2,128)(2,1)} %concatenate.28) | data formatting | bytes 3145728 | tf_op jit(solution)/shard_map/concatenate | solution.py:69
  114.4 0.0 copy-done.2
  114.4 0.0 copy-start.5
  114.4 2.8 %fusion.8 = f32[8,2,512,128,2]{3,2,4,1,0:T(8,128)S(1)} fusion(bf16[8,384,2,128]{3,1,2,0:T(8,128)(2,1)} %copy.14, bf16[8,128,2,128]{3,1,2,0:T(8,128)(2,1)} %copy.13, bf16[8,128,2,2,128]{4,3,2,1,0:T(2,128)(2,1)S(1)} %copy-done.2), kind=kOutput, calls=%fused_computation.18 | convolution fusion | flops 541065216 | bytes 11534336 | tf_op jit(solution)/shard_map/bqgrd,bkgd->bgrqk/dot_general | solution.py:79
  117.3 0.0 copy-done.5
  117.3 0.0 copy-start.3
  117.3 0.0 copy-start.4
  117.3 5.8 %fusion.30 = (f32[8,2,2,128]{3,2,1,0:T(2,128)S(1)}, f32[8,2,2,128,512]{3,4,2,1,0:T(8,128)}) fusion(f32[8,2,512,128,2]{3,2,4,1,0:T(8,128)S(1)} %fusion.8, pred[8,128,512]{1,2,0:T(8,128)(4,1)S(1)} %copy-done.5), kind=kOutput, calls=%fused_computation.63 | output fusion | flops 12583423 | bytes 17317888 | tf_op jit(solution)/shard_map/sub | solution.py:87
  123.0 0.0 copy-done.3
  123.1 0.0 copy-done.4
  123.1 4.3 %fusion.12 = bf16[8,128,2,2,128]{1,4,3,2,0:T(8,128)(2,1)S(1)} fusion(f32[8,2,2,128,512]{3,4,2,1,0:T(8,128)} %get-tuple-element.6, f32[8,2,2,128]{3,2,1,0:T(2,128)S(1)} %get-tuple-element.5, bf16[8,384,2,128]{1,3,2,0:T(8,128)(2,1)S(1)} %copy-done.3, bf16[8,128,2,128]{1,3,2,0:T(8,128)(2,1)S(1)} %copy-done.4), kind=kOutput, calls=%fused_computation.24 | convolution fusion | flops 545783808 | bytes 11550720 | tf_op jit(solution)/shard_map/bgrqk,bkgd->bqgrd/dot_general | solution.py:90
  127.4 0.7 copy.17
  128.1 0.0 copy-done
  128.1 4.3 %convolution_convert_fusion = bf16[1024,2048]{1,0:T(8,128)(2,1)} fusion(bf16[512,2048]{1,0:T(8,128)(2,1)S(1)} %copy-done, bf16[64,8,8,128]{3,2,1,0:T(8,128)(2,1)S(1)} %bitcast.57), kind=kOutput, calls=%fused_computation.13 | convolution fusion | flops 2149580800 | bytes 7340032 | tf_op jit(solution)/shard_map/dot_general | solution.py:98
  132.4 0.0 reduce-scatter.2.cloned.1.call-update
  132.4 45.8 %reduce-scatter.2.cloned.1.call-done = bf16[256,2048]{1,0:T(8,128)(2,1)} async-done(((bf16[1024,2048]{1,0:T(8,128)(2,1)}), bf16[256,2048]{1,0:T(8,128)(2,1)}) %reduce-scatter.2.cloned.1.call-update) | async-done | bytes 1048592 | tf_op jit(solution)/shard_map/reduce_scatter | solution.py:97
  (10 shorter events, 0.1 us)
Async XLA Ops:
  6.5 121.5 %copy-start = (bf16[512,2048]{1,0:T(8,128)(2,1)S(1)}, bf16[512,2048]{1,0:T(8,128)(2,1)}, u32[]{:S(2)}) copy-start(bf16[512,2048]{1,0:T(8,128)(2,1)} %param.10) | copy-start | bytes 6291460
  43.3 1.6 copy-start.1
  44.9 25.1 %all-to-all-start.1 = ((bf16[8,8,32,256]{3,2,1,0:T(8,128)(2,1)}), bf16[8,8,32,256]{3,2,1,0:T(8,128)(2,1)S(1)}, u32[]{:S(2)}, u32[]{:S(2)}) async-start(bf16[8,8,32,256]{3,2,1,0:T(8,128)(2,1)} %bitcast.56), calls=%async_computation.1 | async-start | bytes 2097152 | tf_op jit(solution)/shard_map/all_to_all | solution.py:38
  50.3 24.1 %copy-start.6 = (s32[8,12]{1,0:T(8,128)S(1)}, s32[8,12]{1,0:T(8,128)}, u32[]{:S(2)}) copy-start(s32[8,12]{1,0:T(8,128)} %param.11) | copy-start | bytes 1156
  70.0 32.4 %all-to-all-start = ((bf16[8,8,32,256]{3,2,1,0:T(8,128)(2,1)}), bf16[8,8,32,256]{3,2,1,0:T(8,128)(2,1)}, u32[]{:S(2)}, u32[]{:S(2)}) async-start(bf16[8,8,32,256]{3,2,1,0:T(8,128)(2,1)} %bitcast.55), calls=%async_computation | async-start | bytes 2097152 | tf_op jit(solution)/shard_map/all_to_all | solution.py:39
  74.2 104.1 %reduce-scatter.2.cloned.1.call-start = ((), (), s32[]{:S(2)}) async-start(), calls=%async_computation.3 | async-start | bytes 5242880 | tf_op jit(solution)/shard_map/reduce_scatter | solution.py:97
  102.3 12.1 %copy-start.2 = (bf16[8,128,2,2,128]{4,3,2,1,0:T(2,128)(2,1)S(1)}, bf16[8,128,2,2,128]{4,3,2,1,0:T(2,128)(2,1)}, u32[]{:S(2)}) copy-start(bf16[8,128,2,2,128]{4,3,2,1,0:T(2,128)(2,1)} %reshape.96) | copy-start | bytes 3145732
  114.4 2.8 %copy-start.5 = (pred[8,128,512]{1,2,0:T(8,128)(4,1)S(1)}, pred[8,128,512]{1,2,0:T(8,128)(4,1)}, u32[]{:S(2)}) copy-start(pred[8,128,512]{1,2,0:T(8,128)(4,1)} %compare_and_fusion) | copy-start | bytes 1572868
  117.3 5.8 %copy-start.3 = (bf16[8,384,2,128]{1,3,2,0:T(8,128)(2,1)S(1)}, bf16[8,384,2,128]{1,3,2,0:T(8,128)(2,1)}, u32[]{:S(2)}) copy-start(bf16[8,384,2,128]{1,3,2,0:T(8,128)(2,1)} %copy.12) | copy-start | bytes 4718596
  117.3 5.8 %copy-start.4 = (bf16[8,128,2,128]{1,3,2,0:T(8,128)(2,1)S(1)}, bf16[8,128,2,128]{1,3,2,0:T(8,128)(2,1)}, u32[]{:S(2)}) copy-start(bf16[8,128,2,128]{1,3,2,0:T(8,128)(2,1)} %copy.11) | copy-start | bytes 1572868
Sparse Core Ops, SparseCore 0:
  132.5 45.6 reduce-scatter.1
where the time goes:
time: 186 us; the launch traced here: 185 us
  waiting for transfers between devices  58.3 us (31%)
  local copies, waits for them, and re-layouts  36.5 us (20%)
  blocking collectives  32.7 us (18%)
  matrix products  25.9 us (14%)
  between operations  13.6 us (7%)
  starting transfers between devices  9.92 us (5%)
  other arithmetic  8.31 us (4%)
    reduce_scatter x1, waiting for transfers between devices, shards(): lax.psum_scatter(jnp.dot(mixed, out_weight, preferred_element_type=jnp.fl...  45.8 us
    all_gather x1, blocking collectives, shards(): all_lists = lax.all_gather(chosen, 'kv', axis=0, tiled=True)  32.7 us
    all_to_all x1, waiting for transfers between devices, shards(): lax.all_to_all(key_rows[wanted], 'kv', split_axis=0, concat_axis=0, tiled...  12.4 us
    concatenate x4, local copies, waits for them, and re-layouts, shards(): jnp.concatenate([value_vectors.reshape(query_blocks, QUERY_BLOCK_SPAN, kv...  12.4 us
    concatenate x4, local copies, waits for them, and re-layouts, shards(): jnp.concatenate([key_vectors.reshape(query_blocks, QUERY_BLOCK_SPAN, kv_w...  10.3 us
    dot_general x1, matrix products, shards(): jnp.dot(tokens, query_weight, preferred_element_type=jnp.float32)  6.16 us
    sub x1, other arithmetic, shards(): exp_scores = jnp.exp(scores - row_max)  5.76 us
    all_to_all x1, starting transfers between devices, shards(): lax.all_to_all(key_rows[wanted], 'kv', split_axis=0, concat_axis=0, tiled...  5.46 us
  transfers between devices with their start and end apart: 3, of which 2 were waited for; matrix products, arithmetic and copies ran while one was open for 19% of the time, Pallas kernels for 0%

commit v1 on v0

--- a/solution.py
+++ b/solution.py
@@ -29,7 +29,9 @@
     my_index = lax.axis_index("kv")
     key_rows = key_vectors.reshape(blocked_keys, KEY_BLOCK_SPAN, kv_width)
     value_rows = value_vectors.reshape(blocked_keys, KEY_BLOCK_SPAN, kv_width)
-    all_lists = lax.all_gather(chosen, "kv", axis=0, tiled=True)
+    all_lists = jnp.concatenate(
+        lax.all_to_all(jnp.stack([chosen] * lax.axis_size("kv")), "kv", 0, 0), axis=0
+    )
     peer_count = all_lists.shape[0] // query_blocks
     asked_ids = all_lists.reshape(peer_count, query_blocks, NFAR)
     is_mine = (asked_ids >= 0) & (asked_ids // blocked_keys == my_index)

time: 186 us -> 168 us (0.903)
  blocking collectives: 32.7 us -> 0 us
  waiting for transfers between devices: 58.3 us -> 66.5 us
  starting transfers between devices: 9.92 us -> 15.3 us
    all_gather x1 -> x0, blocking collectives: 32.7 us -> none  [shards(): all_lists = lax.all_gather(chosen, 'kv', axis=0, tiled=True)]
    all_to_all x0 -> x1, starting transfers between devices: none -> 7.28 us  [shards(): lax.all_to_all(jnp.stack([chosen] * lax.axis_size('kv')), 'kv', 0, 0)]
    all_to_all x1, waiting for transfers between devices: 12.4 us -> 17.7 us  [shards(): lax.all_to_all(key_rows[wanted], 'kv', split_axis=0, concat_axis=0, tiled...]
    all_to_all x0 -> x1, waiting for transfers between devices: none -> 2.93 us  [shards(): lax.all_to_all(jnp.stack([chosen] * lax.axis_size('kv')), 'kv', 0, 0)]
    all_to_all x1, starting transfers between devices: 5.46 us -> 3.56 us  [shards(): lax.all_to_all(key_rows[wanted], 'kv', split_axis=0, concat_axis=0, tiled...]
  transfers between devices with their start and end apart: 3 -> 4, of which waited for: 2 -> 3; matrix products, arithmetic and copies ran while one was open for 19% -> 23% of each run, Pallas kernels for 0% -> 0%
where the time goes in v1:
time: 168 us; the launch traced here: 167 us
  waiting for transfers between devices  66.5 us (40%)
  local copies, waits for them, and re-layouts  37.7 us (22%)
  matrix products  25.9 us (15%)
  starting transfers between devices  15.3 us (9%)
  between operations  13.6 us (8%)
  other arithmetic  8.41 us (5%)
    reduce_scatter x1, waiting for transfers between devices, shards(): lax.psum_scatter(jnp.dot(mixed, out_weight, preferred_element_type=jnp.fl...  45.8 us
    all_to_all x1, waiting for transfers between devices, shards(): lax.all_to_all(key_rows[wanted], 'kv', split_axis=0, concat_axis=0, tiled...  17.7 us
    concatenate x4, local copies, waits for them, and re-layouts, shards(): jnp.concatenate([value_vectors.reshape(query_blocks, QUERY_BLOCK_SPAN, kv...  12.3 us
    concatenate x4, local copies, waits for them, and re-layouts, shards(): jnp.concatenate([key_vectors.reshape(query_blocks, QUERY_BLOCK_SPAN, kv_w...  10.3 us
    all_to_all x1, starting transfers between devices, shards(): lax.all_to_all(jnp.stack([chosen] * lax.axis_size('kv')), 'kv', 0, 0)  7.28 us
    dot_general x1, matrix products, shards(): jnp.dot(tokens, query_weight, preferred_element_type=jnp.float32)  6.16 us
    sub x1, other arithmetic, shards(): exp_scores = jnp.exp(scores - row_max)  5.77 us
    dot_general x1, matrix products, shards(): jnp.dot(tokens, value_projection_matrix, preferred_element_type=jnp.float32)  4.56 us
  transfers between devices with their start and end apart: 4, of which 3 were waited for; matrix products, arithmetic and copies ran while one was open for 23% of the time, Pallas kernels for 0%

profile of v1, /device:TPU:0, one launch (start us, length us, event | category | flops | bytes accessed | tf_op | source)
XLA Modules:
  0.0 167.4 jit_solution(2241862337134813320)
XLA Ops:
  6.5 0.0 copy-start
  6.5 1.5 stack.2
  8.0 7.3 %all-to-all-start = ((s32[8,8,12]{2,1,0:T(8,128)}), s32[8,8,12]{2,1,0:T(8,128)S(1)}, u32[]{:S(2)}, u32[]{:S(2)}) async-start(s32[8,8,12]{2,1,0:T(8,128)} %stack.2), calls=%async_computation | async-start | bytes 65536 | tf_op jit(solution)/shard_map/all_to_all | solution.py:33
  15.3 3.7 %convolution_convert_fusion.2 = bf16[1024,256]{1,0:T(8,128)(2,1)S(1)} fusion(bf16[1024,2048]{1,0:T(8,128)(2,1)} %param.6, bf16[2048,256]{1,0:T(8,128)(2,1)} %param.8), kind=kOutput, calls=%fused_computation.25 | convolution fusion | flops 1074003968 | bytes 5767168 | tf_op jit(solution)/shard_map/dot_general | solution.py:23
  19.0 0.0 copy-start.1
  19.0 2.9 %all-to-all-done = s32[8,8,12]{2,1,0:T(8,128)S(1)} async-done(((s32[8,8,12]{2,1,0:T(8,128)}), s32[8,8,12]{2,1,0:T(8,128)S(1)}, u32[]{:S(2)}, u32[]{:S(2)}) %all-to-all-start) | async-done | bytes 3104 | tf_op jit(solution)/shard_map/all_to_all | solution.py:33
  22.0 0.2 select_reduce_fusion
  22.2 0.1 reshape.84
  22.3 1.6 gather_fusion.2
  23.9 0.0 copy-done.1
  23.9 3.6 %all-to-all-start.2 = ((bf16[8,8,32,256]{3,2,1,0:T(8,128)(2,1)}), bf16[8,8,32,256]{3,2,1,0:T(8,128)(2,1)S(1)}, u32[]{:S(2)}, u32[]{:S(2)}) async-start(bf16[8,8,32,256]{3,2,1,0:T(8,128)(2,1)} %bitcast.58), calls=%async_computation.2 | async-start | bytes 2097152 | tf_op jit(solution)/shard_map/all_to_all | solution.py:40
  27.4 0.0 copy-start.6
  27.4 4.6 %convolution_convert_fusion.3 = bf16[1024,256]{1,0:T(8,128)(2,1)} fusion(bf16[1024,2048]{1,0:T(8,128)(2,1)} %param.6, bf16[2048,256]{1,0:T(8,128)(2,1)} %param.9), kind=kOutput, calls=%fused_computation.26 | convolution fusion | flops 1074003968 | bytes 5767168 | tf_op jit(solution)/shard_map/dot_general | solution.py:26
  32.0 2.7 %gather_fusion = bf16[64,32,256]{2,1,0:T(8,128)(2,1)} fusion(bf16[32,32,256]{2,1,0:T(8,128)(2,1)} %bitcast.56, s32[1024]{0:T(1024)S(1)} %pad_clamp_fusion), kind=kCustom, calls=%fused_computation | custom fusion | bytes 2097408 | tf_op jit(solution)/shard_map/gather | solution.py:41
  34.7 17.7 %all-to-all-done.2 = bf16[8,8,32,256]{3,2,1,0:T(8,128)(2,1)S(1)} async-done(((bf16[8,8,32,256]{3,2,1,0:T(8,128)(2,1)}), bf16[8,8,32,256]{3,2,1,0:T(8,128)(2,1)S(1)}, u32[]{:S(2)}, u32[]{:S(2)}) %all-to-all-start.2) | async-done | bytes 1048608 | tf_op jit(solution)/shard_map/all_to_all | solution.py:40
  52.4 4.2 %all-to-all-start.1 = ((bf16[8,8,32,256]{3,2,1,0:T(8,128)(2,1)}), bf16[8,8,32,256]{3,2,1,0:T(8,128)(2,1)}, u32[]{:S(2)}, u32[]{:S(2)}) async-start(bf16[8,8,32,256]{3,2,1,0:T(8,128)(2,1)} %bitcast.57), calls=%async_computation.1 | async-start | bytes 2097152 | tf_op jit(solution)/shard_map/all_to_all | solution.py:41
  56.6 0.2 reduce-scatter.2.cloned.1.call-start
  56.9 0.0 copy-done.6
  56.9 2.0 %concatenate.32 = bf16[8,128,2,128]{3,2,1,0:T(2,128)(2,1)} reshape(bf16[1024,256]{1,0:T(8,128)(2,1)} %copy-done.1) | data formatting | bytes 1048576 | tf_op jit(solution)/shard_map/concatenate | solution.py:64
  58.8 1.9 %concatenate.26 = bf16[8,128,2,128]{3,2,1,0:T(2,128)(2,1)} reshape(bf16[1024,256]{1,0:T(8,128)(2,1)} %convolution_convert_fusion.3) | data formatting | bytes 1048576 | tf_op jit(solution)/shard_map/concatenate | solution.py:71
  60.8 0.1 reshape.90
  60.9 1.9 %copy.20 = bf16[8,128,2,128]{3,1,2,0:T(8,128)(2,1)} copy(bf16[8,128,2,128]{3,2,1,0:T(2,128)(2,1)} %concatenate.32) | data formatting | bytes 1048576 | tf_op jit(solution)/shard_map/concatenate | solution.py:64
  62.8 6.2 %convolution_convert_fusion.1 = bf16[1024,512]{1,0:T(8,128)(2,1)} fusion(bf16[1024,2048]{1,0:T(8,128)(2,1)} %param.6, bf16[2048,512]{1,0:T(8,128)(2,1)} %param.7), kind=kOutput, calls=%fused_computation.23 | convolution fusion | flops 2148007936 | bytes 7340032 | tf_op jit(solution)/shard_map/dot_general | solution.py:22
  69.0 2.2 %reshape.80 = bf16[8,128,2,2,128]{4,3,2,1,0:T(2,128)(2,1)} reshape(bf16[1024,512]{1,0:T(8,128)(2,1)} %convolution_convert_fusion.1) | data formatting | bytes 2097152 | tf_op jit(solution)/shard_map/reshape | solution.py:78
  71.2 0.1 add.60
  71.2 0.1 add.61
  71.3 0.1 add.63
  71.4 0.1 broadcast_in_dim.20
  71.5 0.1 reshape.75
  71.6 1.9 %copy.18 = bf16[8,128,2,128]{1,3,2,0:T(8,128)(2,1)} copy(bf16[8,128,2,128]{3,2,1,0:T(2,128)(2,1)} %concatenate.26) | data formatting | bytes 1048576 | tf_op jit(solution)/shard_map/concatenate | solution.py:71
  73.6 2.4 %compare_and_fusion = pred[8,128,512]{1,2,0:T(8,128)(4,1)} fusion(s32[8,128]{1,0:T(8,128)S(1)} %add_add_fusion, s32[8,512]{1,0:T(8,128)S(1)} %pad_add_fusion, pred[8,512]{1,0:T(8,128)(4,1)S(1)} %concatenate.30), kind=kLoop, calls=%fused_computation.21 | loop fusion | flops 1048576 | bytes 548864 | tf_op jit(solution)/shard_map/and | solution.py:63
  76.0 2.3 %gather_fusion.3 = bf16[96,32,256]{2,1,0:T(8,128)(2,1)} fusion(bf16[8,8,32,256]{3,2,1,0:T(8,128)(2,1)S(1)} %all-to-all-done.2, s32[96]{0:T(128)S(1)} %reshape.90), kind=kCustom, calls=%fused_computation.3 | custom fusion | bytes 3146496 | tf_op jit(solution)/shard_map/gather | solution.py:45
  78.3 3.5 %concatenate.33 = bf16[8,384,2,128]{3,2,1,0:T(2,128)(2,1)} reshape(bf16[96,32,256]{2,1,0:T(8,128)(2,1)} %gather_fusion.3) | data formatting | bytes 3145728 | tf_op jit(solution)/shard_map/concatenate | solution.py:64
  81.8 2.9 %copy.21 = bf16[8,384,2,128]{3,1,2,0:T(8,128)(2,1)} copy(bf16[8,384,2,128]{3,2,1,0:T(2,128)(2,1)} %concatenate.33) | data formatting | bytes 3145728 | tf_op jit(solution)/shard_map/concatenate | solution.py:64
  84.7 0.0 copy-start.2
  84.7 0.0 all-to-all-done.1
  84.7 3.6 %gather_fusion.1 = bf16[96,32,256]{2,1,0:T(8,128)(2,1)} fusion(bf16[8,8,32,256]{3,2,1,0:T(8,128)(2,1)} %all-to-all-done.1, s32[96]{0:T(128)S(1)} %reshape.90), kind=kCustom, calls=%fused_computation.1 | custom fusion | bytes 3146496 | tf_op jit(solution)/shard_map/gather | solution.py:46
  88.3 3.5 %concatenate.28 = bf16[8,384,2,128]{3,2,1,0:T(2,128)(2,1)} reshape(bf16[96,32,256]{2,1,0:T(8,128)(2,1)} %gather_fusion.1) | data formatting | bytes 3145728 | tf_op jit(solution)/shard_map/concatenate | solution.py:71
  91.8 4.9 %copy.19 = bf16[8,384,2,128]{1,3,2,0:T(8,128)(2,1)} copy(bf16[8,384,2,128]{3,2,1,0:T(2,128)(2,1)} %concatenate.28) | data formatting | bytes 3145728 | tf_op jit(solution)/shard_map/concatenate | solution.py:71
  96.7 0.0 copy-done.2
  96.7 0.0 copy-start.5
  96.7 2.8 %fusion.8 = f32[8,2,512,128,2]{3,2,4,1,0:T(8,128)S(1)} fusion(bf16[8,384,2,128]{3,1,2,0:T(8,128)(2,1)} %copy.21, bf16[8,128,2,128]{3,1,2,0:T(8,128)(2,1)} %copy.20, bf16[8,128,2,2,128]{4,3,2,1,0:T(2,128)(2,1)S(1)} %copy-done.2), kind=kOutput, calls=%fused_computation.18 | convolution fusion | flops 541065216 | bytes 11534336 | tf_op jit(solution)/shard_map/bqgrd,bkgd->bgrqk/dot_general | solution.py:81
  99.6 0.0 copy-done.5
  99.6 0.0 copy-start.3
  99.6 0.0 copy-start.4
  99.6 5.8 %fusion.30 = (f32[8,2,2,128]{3,2,1,0:T(2,128)S(1)}, f32[8,2,2,128,512]{3,4,2,1,0:T(8,128)}) fusion(f32[8,2,512,128,2]{3,2,4,1,0:T(8,128)S(1)} %fusion.8, pred[8,128,512]{1,2,0:T(8,128)(4,1)S(1)} %copy-done.5), kind=kOutput, calls=%fused_computation.63 | output fusion | flops 12583423 | bytes 17317888 | tf_op jit(solution)/shard_map/sub | solution.py:89
  105.4 0.0 copy-done.3
  105.4 0.0 copy-done.4
  105.4 4.3 %fusion.12 = bf16[8,128,2,2,128]{1,4,3,2,0:T(8,128)(2,1)S(1)} fusion(f32[8,2,2,128,512]{3,4,2,1,0:T(8,128)} %get-tuple-element.6, f32[8,2,2,128]{3,2,1,0:T(2,128)S(1)} %get-tuple-element.5, bf16[8,384,2,128]{1,3,2,0:T(8,128)(2,1)S(1)} %copy-done.3, bf16[8,128,2,128]{1,3,2,0:T(8,128)(2,1)S(1)} %copy-done.4), kind=kOutput, calls=%fused_computation.24 | convolution fusion | flops 545783808 | bytes 11550720 | tf_op jit(solution)/shard_map/bgrqk,bkgd->bqgrd/dot_general | solution.py:92
  109.7 0.7 copy.24
  110.4 0.0 copy-done
  110.4 4.3 %convolution_convert_fusion = bf16[1024,2048]{1,0:T(8,128)(2,1)} fusion(bf16[512,2048]{1,0:T(8,128)(2,1)S(1)} %copy-done, bf16[64,8,8,128]{3,2,1,0:T(8,128)(2,1)S(1)} %bitcast.59), kind=kOutput, calls=%fused_computation.13 | convolution fusion | flops 2149580800 | bytes 7340032 | tf_op jit(solution)/shard_map/dot_general | solution.py:100
  114.7 0.0 reduce-scatter.2.cloned.1.call-update
  114.7 45.8 %reduce-scatter.2.cloned.1.call-done = bf16[256,2048]{1,0:T(8,128)(2,1)} async-done(((bf16[1024,2048]{1,0:T(8,128)(2,1)}), bf16[256,2048]{1,0:T(8,128)(2,1)}) %reduce-scatter.2.cloned.1.call-update) | async-done | bytes 1048592 | tf_op jit(solution)/shard_map/reduce_scatter | solution.py:99
  (10 shorter events, 0.1 us)
Async XLA Ops:
  6.5 103.9 %copy-start = (bf16[512,2048]{1,0:T(8,128)(2,1)S(1)}, bf16[512,2048]{1,0:T(8,128)(2,1)}, u32[]{:S(2)}) copy-start(bf16[512,2048]{1,0:T(8,128)(2,1)} %param.10) | copy-start | bytes 6291460
  8.0 14.0 %all-to-all-start = ((s32[8,8,12]{2,1,0:T(8,128)}), s32[8,8,12]{2,1,0:T(8,128)S(1)}, u32[]{:S(2)}, u32[]{:S(2)}) async-start(s32[8,8,12]{2,1,0:T(8,128)} %stack.2), calls=%async_computation | async-start | bytes 65536 | tf_op jit(solution)/shard_map/all_to_all | solution.py:33
  19.0 4.9 %copy-start.1 = (bf16[1024,256]{1,0:T(8,128)(2,1)}, bf16[1024,256]{1,0:T(8,128)(2,1)S(1)}, u32[]{:S(2)}) copy-start(bf16[1024,256]{1,0:T(8,128)(2,1)S(1)} %convolution_convert_fusion.2) | copy-start | bytes 1572868
  23.9 28.5 %all-to-all-start.2 = ((bf16[8,8,32,256]{3,2,1,0:T(8,128)(2,1)}), bf16[8,8,32,256]{3,2,1,0:T(8,128)(2,1)S(1)}, u32[]{:S(2)}, u32[]{:S(2)}) async-start(bf16[8,8,32,256]{3,2,1,0:T(8,128)(2,1)} %bitcast.58), calls=%async_computation.2 | async-start | bytes 2097152 | tf_op jit(solution)/shard_map/all_to_all | solution.py:40
  27.4 29.4 %copy-start.6 = (s32[8,12]{1,0:T(8,128)S(1)}, s32[8,12]{1,0:T(8,128)}, u32[]{:S(2)}) copy-start(s32[8,12]{1,0:T(8,128)} %param.11) | copy-start | bytes 1156
  52.4 32.3 %all-to-all-start.1 = ((bf16[8,8,32,256]{3,2,1,0:T(8,128)(2,1)}), bf16[8,8,32,256]{3,2,1,0:T(8,128)(2,1)}, u32[]{:S(2)}, u32[]{:S(2)}) async-start(bf16[8,8,32,256]{3,2,1,0:T(8,128)(2,1)} %bitcast.57), calls=%async_computation.1 | async-start | bytes 2097152 | tf_op jit(solution)/shard_map/all_to_all | solution.py:41
  56.6 104.0 %reduce-scatter.2.cloned.1.call-start = ((), (), s32[]{:S(2)}) async-start(), calls=%async_computation.4 | async-start | bytes 5242880 | tf_op jit(solution)/shard_map/reduce_scatter | solution.py:99
  84.7 12.1 %copy-start.2 = (bf16[8,128,2,2,128]{4,3,2,1,0:T(2,128)(2,1)S(1)}, bf16[8,128,2,2,128]{4,3,2,1,0:T(2,128)(2,1)}, u32[]{:S(2)}) copy-start(bf16[8,128,2,2,128]{4,3,2,1,0:T(2,128)(2,1)} %reshape.80) | copy-start | bytes 3145732
  96.7 2.8 %copy-start.5 = (pred[8,128,512]{1,2,0:T(8,128)(4,1)S(1)}, pred[8,128,512]{1,2,0:T(8,128)(4,1)}, u32[]{:S(2)}) copy-start(pred[8,128,512]{1,2,0:T(8,128)(4,1)} %compare_and_fusion) | copy-start | bytes 1572868
  99.6 5.8 %copy-start.3 = (bf16[8,384,2,128]{1,3,2,0:T(8,128)(2,1)S(1)}, bf16[8,384,2,128]{1,3,2,0:T(8,128)(2,1)}, u32[]{:S(2)}) copy-start(bf16[8,384,2,128]{1,3,2,0:T(8,128)(2,1)} %copy.19) | copy-start | bytes 4718596
  99.6 5.8 %copy-start.4 = (bf16[8,128,2,128]{1,3,2,0:T(8,128)(2,1)S(1)}, bf16[8,128,2,128]{1,3,2,0:T(8,128)(2,1)}, u32[]{:S(2)}) copy-start(bf16[8,128,2,128]{1,3,2,0:T(8,128)(2,1)} %copy.18) | copy-start | bytes 1572868
Sparse Core Ops, SparseCore 0:
  114.9 45.6 reduce-scatter.1
